TPU v7x, 32 devices: a whole 2x2x4 slice. The times are simulated.
32 devices in a mesh: ep: 32 (over z, y, x, core).
Axes of the slice: x: 2, y: 2, z: 4, core: 2. Of those that a mesh axis runs over, the one named last changes fastest.
Arguments:
- tokens: bfloat16 [2048, 2048], P('ep'), may hold values from -6 to 6
- conv_state: bfloat16 [2048, 3, 1024], P('ep'), may hold values from -6 to 6
- recur_state: float32 [2048, 1024], P('ep'), may hold values from -6 to 6
- w_branch: bfloat16 [2048, 1024], replicated, may hold values from -0.125 to 0.125
- w_gate: bfloat16 [2048, 1024], replicated, may hold values from -0.125 to 0.125
- conv_taps: float32 [4, 1024], replicated, may hold values from -3 to 3
- rate_blocks: bfloat16 [16, 64, 64], replicated, may hold values from -0.75 to 0.75
- input_blocks: bfloat16 [16, 64, 64], replicated, may hold values from -0.75 to 0.75
- decay_param: float32 [1024], replicated, may hold values from 1.5 to 6.5
- w_mix: bfloat16 [1024, 2048], replicated, may hold values from -0.1875 to 0.1875
- gain_pre: float32 [2048], replicated, may hold values from 0.1 to 1.9
- gain_post: float32 [2048], replicated, may hold values from 0.1 to 1.9
- gain_ffn: float32 [2048], replicated, may hold values from 0.1 to 1.9
- gain_out: float32 [2048], replicated, may hold values from 0.1 to 1.9
- routes: int32 [2048, 2], P('ep'), may hold values from 0 to 31, all different within a row; in each aligned block of 64 rows (0 to 63, 64 to 127, ...) at most 12 rows name the same one
- affinity: float32 [2048, 2], P('ep'), may hold values from 0.05 to 1
- w_expert_gate: bfloat16 [32, 2048, 512], P('ep'), may hold values from -0.125 to 0.125
- w_expert_up: bfloat16 [32, 2048, 512], P('ep'), may hold values from -0.125 to 0.125
- w_expert_down: bfloat16 [32, 512, 2048], P('ep'), may hold values from -0.25 to 0.25
Outputs:
- layer_out: bfloat16 [2048, 2048], P('ep')
- conv_next: bfloat16 [2048, 3, 1024], P('ep')
- state_next: float32 [2048, 1024], P('ep')
Inputs may be any that keep to these rules, and one draw needn't show every extreme that they name: `routes`: each row names 2 different experts. Among the 64 rows of one device no expert is named more than 12 times, and in every draw some device names some expert exactly 12 times.
All inputs are finite; a program needn't handle non-finite values.
Results may differ from a plain program's by a relative error of at most 0.014.
Values may be sent and summed in bfloat16 or wider, within the bound.
A program may use at most 128 MiB of HBM per device.

v0:
```python
import functools

import jax
import jax.numpy as jnp
from jax import lax
from jax.experimental import pallas as pl
from jax.experimental.pallas import tpu as pltpu
from jax.sharding import PartitionSpec as P

epsilon = 1e-06
gate_scale = 8.0
planes = 4
chunks = 4


def rms(values, gain):
    return values * lax.rsqrt(jnp.mean(values * values, axis=-1, keepdims=True) + epsilon) * gain


def layer_kernel(
    n, capacity, limit, top,
    tokens, pre, taps, recur, rate_b, input_b, decay_p, g_pre, g_post, g_ffn, g_out, routes, affinity,
    wb_hbm, wg_hbm, wm_hbm, eg_hbm, eu_hbm, ed_hbm,
    out, branch_out, state_out,
    wb, wg, wm, normed, gate_act, merged, mix, residual, message, mall,
    eg, eu, ed, xall, sbuf, rbuf, obuf, cbuf, pbuf, fbuf, total,
    load_sem, ms, mr, zs, zr, ds_, dr, os_, orr, ps, pr,
):
    parts, lots, part = xall.shape
    group = n // planes
    slots = rbuf.shape[1]
    slab = slots // group
    me = lax.axis_index("ep")
    plane, column = me // group, lax.rem(me, group)
    rows, width = tokens.shape
    channels = pre.shape[1]
    block = rate_b.shape[1]
    loads = [
        pltpu.make_async_copy(src, dst, load_sem.at[k])
        for k, (src, dst) in enumerate(
            (
                (wb_hbm, wb), (wg_hbm, wg), (wm_hbm, wm),
                (eg_hbm.at[0], eg), (eu_hbm.at[0], eu), (ed_hbm.at[0], ed),
            )
        )
    ]
    for load in loads:
        load.start()

    barrier = pltpu.get_barrier_semaphore()

    @pl.loop(1, n)
    def _(d):
        pl.semaphore_signal(barrier, inc=1, device_id={"ep": lax.rem(me + d, n)})

    normed[...] = rms(tokens[...].astype(jnp.float32), g_pre[...]).astype(jnp.bfloat16)
    tile = 256
    loads[0].wait()

    @pl.loop(0, channels // tile)
    def _(t):
        cols = pl.ds(pl.multiple_of(t * tile, tile), tile)
        branch_out[:, cols] = jnp.dot(
            normed[...], wb[:, cols], preferred_element_type=jnp.float32
        ).astype(jnp.bfloat16)

    def lanes(k):
        return pl.ds(pl.multiple_of(k * message.shape[1], message.shape[1]), message.shape[1])

    def message_copy(d, landing):
        device = lax.rem(me + d, n)
        spot = device if landing else me
        return pltpu.make_async_remote_copy(
            src_ref=message, dst_ref=mall.at[:, lanes(spot)], send_sem=ms.at[device],
            recv_sem=mr.at[spot], device_id={"ep": device},
            device_id_type=pl.DeviceIdType.MESH,
        )

    spots = lax.broadcasted_iota(jnp.int32, (rows, message.shape[1]), 1)
    wide = jnp.full((rows, message.shape[1]), -1.0, jnp.float32)
    for k in range(top):
        wide = jnp.where(spots == k, routes[:, k : k + 1].astype(jnp.float32), wide)
        wide = jnp.where(spots == top + k, affinity[:, k : k + 1], wide)
    message[...] = jnp.full(message.shape, -1.0, jnp.float32)
    message[:, :rows] = jnp.transpose(wide)[: message.shape[0]]
    pl.semaphore_wait(barrier, n - 1)

    @pl.loop(1, n)
    def _(d):
        message_copy(d, False).start()

    mall[:, lanes(me)] = message[...]
    loads[1].wait()

    @pl.loop(0, channels // tile)
    def _(t):
        cols = pl.ds(pl.multiple_of(t * tile, tile), tile)
        gate_act[:, cols] = jnp.dot(
            normed[...], wg[:, cols], preferred_element_type=jnp.float32
        ).astype(jnp.bfloat16)

    same = lax.broadcasted_iota(jnp.int32, (tile, tile), 0) // block == (
        lax.broadcasted_iota(jnp.int32, (tile, tile), 1) // block
    )

    def spread(ref, t):
        part = ref[pl.ds(t * tile, tile), :].astype(jnp.float32)
        return jnp.where(same, jnp.concatenate([part] * (tile // block), axis=1), 0.0).astype(
            jnp.bfloat16
        )

    for t in range(channels // tile):
        cols = pl.ds(t * tile, tile)
        conv = pre[:, cols] + branch_out[:, cols].astype(jnp.float32) * taps[taps.shape[0] - 1 :, cols]
        conv16 = conv.astype(jnp.bfloat16)
        rate = jax.nn.sigmoid(
            jnp.dot(conv16, spread(rate_b, t), preferred_element_type=jnp.float32)
        )
        inflow = jax.nn.sigmoid(
            jnp.dot(conv16, spread(input_b, t), preferred_element_type=jnp.float32)
        )
        log_decay = rate * (-gate_scale * jax.nn.softplus(-decay_p[:, cols]))
        decay = jnp.exp(log_decay)
        rest = -jnp.tanh(log_decay) * (decay * decay + 1.0)
        state = decay * recur[:, cols] + jnp.sqrt(rest) * (inflow * conv)
        state_out[:, cols] = state
        merged[:, cols] = (state * jax.nn.gelu(gate_act[:, cols].astype(jnp.float32))).astype(
            jnp.bfloat16
        )
    loads[2].wait()

    @pl.loop(0, width // tile)
    def _(t):
        cols = pl.ds(pl.multiple_of(t * tile, tile), tile)
        mix[:, cols] = (
            jnp.dot(merged[...], wm[:, cols], preferred_element_type=jnp.float32)
            .astype(jnp.bfloat16)
            .astype(jnp.float32)
        )

    residual[...] = tokens[...].astype(jnp.float32) + rms(mix[...], g_post[...])
    ffn = rms(residual[...], g_ffn[...]).astype(jnp.bfloat16)
    own = pl.ds(pl.multiple_of(plane * rows, rows), rows)
    for c in range(parts):
        xall[c, own] = ffn[:, c * part : (c + 1) * part]

    def along(d):
        other = lax.rem(plane + d, planes)
        return other, other * group + column

    def beside(d):
        other = lax.rem(column + d, group)
        return other, plane * group + other

    def rcopy(src, dst, send, recv, device):
        return pltpu.make_async_remote_copy(
            src_ref=src, dst_ref=dst, send_sem=send, recv_sem=recv,
            device_id={"ep": device}, device_id_type=pl.DeviceIdType.MESH,
        )

    def strip(k):
        return pl.ds(pl.multiple_of(k * slab, slab), slab)

    def seqs(k):
        return pl.ds(pl.multiple_of(k * rows, rows), rows)

    def token_hop(c, origin, up):
        return rcopy(
            xall.at[c, seqs(origin)], xall.at[c, seqs(origin)],
            zs.at[c, origin + (planes if up else 0)], zr.at[c, origin],
            lax.rem(me + (group if up else n - group), n),
        )

    def each_hop(c, step):
        for up in (True, False):
            open_end = plane + 1 < planes if up else plane > 0
            for h in range(planes):
                origin = plane - h if up else plane + h
                held = origin >= 0 if up else origin < planes

                @pl.when(open_end & held)
                def _():
                    step(token_hop(c, origin, up))

    def own_hops(c):
        for up in (True, False):

            @pl.when(plane + 1 < planes if up else plane > 0)
            def _():
                token_hop(c, plane, up).start()

    def pass_on(c):
        for h in range(1, planes):
            for up in (True, False):
                origin = plane - h if up else plane + h

                @pl.when(origin >= 0 if up else origin < planes)
                def _():
                    token_hop(c, origin, up).wait_recv()

                    @pl.when(plane + 1 < planes if up else plane > 0)
                    def _():
                        token_hop(c, origin, up).start()

    def slab_copy(c, d, landing, src, dst, send, recv):
        other, device = beside(d)
        spot = other if landing else column
        return rcopy(
            src.at[c, strip(other)], dst.at[c, strip(spot)], send.at[c, other],
            recv.at[c, spot], device,
        )

    def back_copy(c, d, landing):
        other, device = along(d)
        spot = other if landing else plane
        return rcopy(
            pbuf.at[c, seqs(other)], fbuf.at[c, seqs(spot)], ps.at[c, other],
            pr.at[c, spot], device,
        )

    far = list(range(1, planes))
    near = list(range(1, group))
    ahead = 2
    for c in range(min(ahead, parts)):
        own_hops(c)

    @pl.loop(1, n)
    def _(d):
        message_copy(d, True).wait_recv()

    f32 = jnp.float32
    names = lax.broadcasted_iota(jnp.int32, (group, 1), 0)
    named = (names + plane * group).astype(f32)
    every = jnp.zeros((group, mall.shape[1]), f32)
    for k in range(top):
        every = every + jnp.where(mall[k : k + 1, :] == named, 1.0, 0.0)
    device_at = lax.broadcasted_iota(jnp.int32, every.shape, 1) // message.shape[1]
    lot_at = lax.broadcasted_iota(jnp.int32, (1, lots), 1)
    base = jnp.zeros((group, lots), f32)
    current = []
    for q in range(planes):
        device = q * group + column
        before = jnp.sum(jnp.where(device_at < device, every, 0.0), axis=1, keepdims=True)
        base = jnp.where(lot_at // rows == q, before, base)
        current.append(mall[:, lanes(device)][:, :rows])
    current = jnp.concatenate(current, axis=1)
    one = [jnp.where(current[k : k + 1, :] == named, 1.0, 0.0) for k in range(top)]
    left = lax.broadcasted_iota(jnp.int32, (lots, lots), 0)
    right = lax.broadcasted_iota(jnp.int32, (lots, lots), 1)
    upper = jnp.where((left // rows == right // rows) & (left < right), 1.0, 0.0)
    slot = jnp.dot(
        sum(one).astype(jnp.bfloat16), upper.astype(jnp.bfloat16), preferred_element_type=f32
    )
    spot_of = jnp.where(
        base + slot < limit,
        (names * slab + (lot_at // rows) * capacity + 1).astype(f32) + slot,
        0.0,
    )
    codes = [jnp.sum(one[k] * spot_of, axis=0, keepdims=True) - 1.0 for k in range(top)]
    raw = [current[top + k : top + k + 1, :] for k in range(top)]
    shares = [r / sum(raw) for r in raw]
    spare = [jnp.zeros((1, lots), f32)] * (-2 * top % 8)
    turned = jnp.transpose(jnp.concatenate(codes + shares + spare, axis=0))

    row_at = lax.broadcasted_iota(jnp.int32, (slots, lots), 0).astype(f32)
    pick = jnp.zeros((slots, lots), f32)
    for k in range(top):
        pick = jnp.where(row_at == codes[k], 1.0, pick)
    pick = pick.astype(jnp.bfloat16)
    col_at = lax.broadcasted_iota(jnp.int32, (lots, slots), 1).astype(f32)
    blend = jnp.zeros((lots, slots), f32)
    for k in range(top):
        blend = jnp.where(
            col_at == turned[:, k : k + 1], turned[:, top + k : top + k + 1], blend
        )
    high = blend.astype(jnp.bfloat16)
    low = (blend - high.astype(f32)).astype(jnp.bfloat16)

    sums = [None, None]

    def absorb(c):
        for d in near:
            slab_copy(c, d, True, sbuf, rbuf, ds_, dr).wait_recv()
        got = rbuf[c]
        for k, w in enumerate((eg, eu)):
            piece = jnp.dot(
                got, w[c * part : (c + 1) * part, :], preferred_element_type=jnp.float32
            )
            sums[k] = piece if sums[k] is None else sums[k] + piece

    for c in range(parts):
        pass_on(c)
        if c + ahead < parts:
            own_hops(c + ahead)
        sbuf[c] = jnp.dot(pick, xall[c], preferred_element_type=jnp.float32).astype(jnp.bfloat16)
        for d in near:
            slab_copy(c, d, False, sbuf, rbuf, ds_, dr).start()
        rbuf[c, strip(column)] = sbuf[c, strip(column)]
        if c == 0:
            for load in loads[3:]:
                load.wait()
        else:
            absorb(c - 1)
    absorb(parts - 1)
    hidden = (jax.nn.silu(sums[0]) * sums[1]).astype(jnp.bfloat16)

    for c in range(parts):
        obuf[c] = jnp.dot(
            hidden, ed[:, c * part : (c + 1) * part], preferred_element_type=jnp.float32
        ).astype(jnp.bfloat16)
        for d in near:
            slab_copy(c, d, False, obuf, cbuf, os_, orr).start()
        cbuf[c, strip(column)] = obuf[c, strip(column)]

    for c in range(parts):
        for d in near:
            slab_copy(c, d, True, obuf, cbuf, os_, orr).wait_recv()
        got = cbuf[c]
        pbuf[c] = (
            jnp.dot(high, got, preferred_element_type=jnp.float32)
            + jnp.dot(low, got, preferred_element_type=jnp.float32)
        ).astype(jnp.bfloat16)
        for d in far:
            back_copy(c, d, False).start()
        fbuf[c, seqs(plane)] = pbuf[c, seqs(plane)]

    squares = jnp.zeros((rows, 1), jnp.float32)
    for c in range(parts):
        for d in far:
            back_copy(c, d, True).wait_recv()
        summed = fbuf[c, 0:rows].astype(jnp.float32)
        for q in range(1, planes):
            summed = summed + fbuf[c, q * rows : (q + 1) * rows].astype(jnp.float32)
        total[c] = summed
        squares = squares + jnp.sum(summed * summed, axis=1, keepdims=True)
    scale = lax.rsqrt(squares / (parts * part) + epsilon)
    for c in range(parts):
        cols = slice(c * part, (c + 1) * part)
        out[:, cols] = (residual[:, cols] + total[c] * scale * g_out[:, cols]).astype(out.dtype)

    @pl.loop(1, n)
    def _(d):
        message_copy(d, False).wait_send()

    for c in range(parts):
        each_hop(c, lambda hop: hop.wait_send())
        for d in far:
            back_copy(c, d, False).wait_send()
        for d in near:
            slab_copy(c, d, False, sbuf, rbuf, ds_, dr).wait_send()
            slab_copy(c, d, False, obuf, cbuf, os_, orr).wait_send()


def vmem(count):
    return [pl.BlockSpec(memory_space=pltpu.VMEM)] * count


def anywhere(count):
    return [pl.BlockSpec(memory_space=pl.ANY)] * count


def shards(
    tokens, conv_state, recur_state, w_branch, w_gate, conv_taps, rate_blocks, input_blocks,
    decay_param, w_mix, gain_pre, gain_post, gain_ffn, gain_out, routes, affinity,
    w_expert_gate, w_expert_up, w_expert_down,
):
    n = lax.axis_size("ep")
    rows, width = tokens.shape
    channels = recur_state.shape[1]
    top = routes.shape[1]
    hidden = w_expert_gate.shape[2]
    bf16, f32 = jnp.bfloat16, jnp.float32
    group = n // planes
    capacity = max(2, 3 * rows * top // n)
    limit = rows * top // 2
    slab = -(-planes * capacity // 16) * 16
    slots, lots, part = group * slab, planes * rows, width // chunks

    row = lambda v: v.reshape(1, -1)
    pre = jnp.sum(conv_state.astype(f32) * conv_taps[None, :-1], axis=1)
    letter = (-(-2 * top // 8) * 8, -(-rows // 128) * 128)
    block = rate_blocks.shape[1]
    dma = lambda *count: pltpu.SemaphoreType.DMA(count)
    layer_out, branch, state_next = pl.pallas_call(
        functools.partial(layer_kernel, n, capacity, limit, top),
        out_shape=(
            jax.ShapeDtypeStruct((rows, width), bf16),
            jax.ShapeDtypeStruct((rows, channels), bf16),
            jax.ShapeDtypeStruct((rows, channels), f32),
        ),
        in_specs=vmem(13) + anywhere(6),
        out_specs=tuple(vmem(3)),
        scratch_shapes=[
            pltpu.VMEM((width, channels), bf16),
            pltpu.VMEM((width, channels), bf16),
            pltpu.VMEM((channels, width), bf16),
            pltpu.VMEM((rows, width), bf16),
            pltpu.VMEM((rows, channels), bf16),
            pltpu.VMEM((rows, channels), bf16),
            pltpu.VMEM((rows, width), f32),
            pltpu.VMEM((rows, width), f32),
            pltpu.VMEM(letter, f32),
            pltpu.VMEM((letter[0], n * letter[1]), f32),
            pltpu.VMEM((width, hidden), bf16),
            pltpu.VMEM((width, hidden), bf16),
            pltpu.VMEM((hidden, width), bf16),
            pltpu.VMEM((chunks, lots, part), bf16),
            pltpu.VMEM((chunks, slots, part), bf16),
            pltpu.VMEM((chunks, slots, part), bf16),
            pltpu.VMEM((chunks, slots, part), bf16),
            pltpu.VMEM((chunks, slots, part), bf16),
            pltpu.VMEM((chunks, lots, part), bf16),
            pltpu.VMEM((chunks, lots, part), bf16),
            pltpu.VMEM((chunks, rows, part), f32),
            dma(6), dma(n), dma(n),
            dma(chunks, 2 * planes), dma(chunks, planes), dma(chunks, group), dma(chunks, group),
            dma(chunks, group), dma(chunks, group), dma(chunks, planes), dma(chunks, planes),
        ],
        compiler_params=pltpu.CompilerParams(
            collective_id=0, has_side_effects=True, vmem_limit_bytes=60 << 20
        ),
    )(
        tokens, pre, conv_taps, recur_state, rate_blocks.reshape(channels, block),
        input_blocks.reshape(channels, block), row(decay_param), row(gain_pre), row(gain_post),
        row(gain_ffn), row(gain_out), routes, affinity,
        w_branch, w_gate, w_mix, w_expert_gate, w_expert_up, w_expert_down,
    )
    conv_next = jnp.concatenate([conv_state[:, 1:], branch[:, None, :]], axis=1)
    return (layer_out, conv_next, state_next)


def solution(mesh):
    ep, copied = "ep", P()
    return jax.shard_map(
        shards,
        mesh=mesh,
        in_specs=(P(ep, None), P(ep, None, None), P(ep, None))
        + (copied,) * 11
        + (P(ep, None),) * 2
        + (P(ep, None, None),) * 3,
        out_specs=(P(ep, None), P(ep, None, None), P(ep, None)),
        check_vma=False,
    )
```

profile of v0, /device:TPU:0, one launch (start us, length us, event | category | flops | bytes accessed | tf_op | source)
XLA Modules:
  0.0 87.4 jit_solution(4617836840365076555)
XLA Ops:
  0.6 1.4 %copy.22.routes = s32[64,2]{1,0:T(8,128)} copy(s32[64,2]{0,1:T(2,128)} %param.33) | data formatting | bytes 1024 | tf_op args[14]
  2.0 1.4 %copy.23.affinity = f32[64,2]{1,0:T(8,128)} copy(f32[64,2]{0,1:T(2,128)} %param.34) | data formatting | bytes 1024 | tf_op args[15]
  3.4 1.8 %multiply_reduce_fusion.pre = f32[64,1024]{1,0:T(8,128)} fusion(bf16[64,3,1024]{2,0,1:T(8,128)(2,1)} %param.20, f32[3,1024]{1,0:T(4,128)} %bitcast.12), kind=kLoop, calls=%fused_computation | loop fusion | flops 524288 | bytes 667648 | tf_op jit(solution)/shard_map/reduce_sum | solution.py:380
  5.2 0.0 slice-start
  5.2 77.1 %shard_map.202 = (bf16[64,2048]{1,0:T(8,128)(2,1)}, bf16[64,1024]{1,0:T(8,128)(2,1)}, f32[64,1024]{1,0:T(8,128)}) custom-call(bf16[64,2048]{1,0:T(8,128)(2,1)} %tokens.1, f32[64,1024]{1,0:T(8,128)} %multiply_reduce_fusion.pre, f32[4,1024]{1,0:T(4,128)} %taps.1, f32[64,1024]{1,0:T(8,128)} %recur.1, bf16[1024,64]{1,0:T(8,128)(2,1)} %bitcast.9, ...), custom_call_target="tpu_custom_call" | custom-call | tf_op jit(solution)/shard_map/pallas_call | solution.py:384
  82.3 0.0 slice-done
  82.4 1.7 %pad_maximum_fusion = bf16[64,3,1024]{2,0,1:T(8,128)(2,1)} fusion(bf16[64,1,1024]{2,0,1:T(8,128)(2,1)} %bitcast.11, bf16[64,2,1024]{2,0,1:T(8,128)(2,1)S(1)} %slice-done), kind=kLoop, calls=%fused_computation.1 | loop fusion | flops 196608 | bytes 786432 | tf_op jit(solution)/shard_map/concatenate | solution.py:428
  84.0 1.7 %copy.26 = bf16[64,2048]{1,0:T(8,128)(2,1)} copy(bf16[64,2048]{1,0:T(8,128)(2,1)} %get-tuple-element.12) | data formatting | bytes 524288
  85.7 1.7 %copy.27 = f32[64,1024]{1,0:T(8,128)} copy(f32[64,1024]{1,0:T(8,128)} %get-tuple-element.14) | data formatting | bytes 524288
Async XLA Ops:
  5.2 77.1 %slice-start = ((bf16[64,3,1024]{2,0,1:T(8,128)(2,1)}), bf16[64,2,1024]{2,0,1:T(8,128)(2,1)S(1)}, s32[]{:S(2)}) async-start(bf16[64,3,1024]{2,0,1:T(8,128)(2,1)} %param.20), calls=%async_computation | async-start | bytes 524288 | tf_op jit(solution)/shard_map/slice | solution.py:428
where the time goes:
time: 87.7 us; the launch traced here: 87.4 us
  Pallas kernels  77.1 us (88%)
  local copies, waits for them, and re-layouts  6.11 us (7%)
  other arithmetic  3.49 us (4%)
    pallas_call x1, Pallas kernels, shards(): pl.pallas_call(functools.partial(layer_kernel, n, capacity, limit, top),...  77.1 us
    unnamed x4, local copies, waits for them, and re-layouts  6.1 us
    reduce_sum x1, other arithmetic, shards(): pre = jnp.sum(conv_state.astype(f32) * conv_taps[None, :-1], axis=1)  1.8 us

commit v1 on v0

v1 whole, which is shorter than its diff:
```python
import functools

import jax
import jax.numpy as jnp
from jax import lax
from jax.experimental import pallas as pl
from jax.experimental.pallas import tpu as pltpu
from jax.sharding import PartitionSpec as P

epsilon = 1e-06
gate_scale = 8.0
planes = 4
cores = 2
steps = 4
tile = 256
lane = 128

f32, bf16 = jnp.float32, jnp.bfloat16


def rms(values, gain):
    return values * lax.rsqrt(jnp.mean(values * values, axis=-1, keepdims=True) + epsilon) * gain


def iota(shape, dim):
    return lax.broadcasted_iota(jnp.int32, shape, dim)


class Exchange:
    def __init__(self, n, refs):
        (
            self.zb, self.ob, self.ib, self.pb, self.sb, self.lo, self.hi, self.m1, self.m2,
            self.zs, self.zr, self.zds, self.zdr, self.os, self.ir,
            self.ps, self.pr, self.pds, self.pdr, self.ss, self.lr, self.hr,
        ) = refs
        self.n = n
        self.group = n // planes
        self.chips = self.group // cores
        me = lax.axis_index("ep")
        self.me = me
        self.plane, column = me // self.group, lax.rem(me, self.group)
        self.chip, self.core = column // cores, lax.rem(column, cores)
        self.partner = me - self.core + lax.rem(self.core + 1, cores)

    def rcopy(self, src, dst, send, recv, device):
        return pltpu.make_async_remote_copy(
            src_ref=src, dst_ref=dst, send_sem=send, recv_sem=recv,
            device_id={"ep": device}, device_id_type=pl.DeviceIdType.MESH,
        )

    def put_z(self, j, rows):
        self.zb[j, self.core, self.plane] = rows
        for up in (True, False):

            @pl.when(self.plane + 1 < planes if up else self.plane > 0)
            def _():
                self.z_copy(j, self.plane, up).start()

    def put_p(self, j, rows):
        self.pb[j, self.core, self.chip] = rows
        for d in range(1, self.chips):
            self.p_copy(j, d).start()

    def z_copy(self, j, origin, up):
        spot = self.zb.at[j, self.core, origin]
        return self.rcopy(
            spot, spot, self.zs.at[j, origin + (planes if up else 0)], self.zr.at[j, origin],
            lax.rem(self.me + (self.group if up else self.n - self.group), self.n),
        )

    def z_hop(self, j, h):
        for up in (True, False):
            origin = self.plane - h if up else self.plane + h

            @pl.when(origin >= 0 if up else origin < planes)
            def _():
                self.z_copy(j, origin, up).wait_recv()

                @pl.when(self.plane + 1 < planes if up else self.plane > 0)
                def _():
                    self.z_copy(j, origin, up).start()

    def z_share_copy(self, j, landing):
        core = lax.rem(self.core + 1, cores) if landing else self.core
        spot = self.zb.at[j, core]
        return self.rcopy(spot, spot, self.zds.at[j], self.zdr.at[j], self.partner)

    def z_share(self, j):
        self.z_share_copy(j, False).start()

    def beside(self, d):
        other = lax.rem(self.chip + d, self.chips)
        return other, self.plane * self.group + other * cores + self.core

    def o_copy(self, j, d):
        other, device = self.beside(d)
        return self.rcopy(
            self.ob.at[j, other], self.ib.at[j, self.chip], self.os.at[j], self.ir.at[j], device
        )

    def o_all(self, j):
        most = pl.ds(0, self.chips - 1)
        return self.rcopy(
            self.ob.at[j, most], self.ib.at[j, most], self.os.at[j], self.ir.at[j], self.partner
        )

    def z_mix(self, j):
        self.z_share_copy(j, True).wait_recv()
        rows, width = self.zb.shape[-2:]
        mixed = jnp.dot(
            self.m1[...], self.zb[j].reshape(-1, width), preferred_element_type=f32
        ).astype(bf16)
        self.ob[j] = mixed.reshape(self.chips, rows, width)
        for d in range(1, self.chips):
            self.o_copy(j, d).start()
        self.ib[j, self.chip] = self.ob[j, self.chip]

    def z_take(self, j):
        self.o_all(j).wait_recv()
        total = self.ib[j, 0].astype(f32)
        for chip in range(1, self.chips):
            total = total + self.ib[j, chip].astype(f32)
        return total

    def p_copy(self, j, d):
        _, device = self.beside(d)
        spot = self.pb.at[j, self.core, self.chip]
        return self.rcopy(spot, spot, self.ps.at[j], self.pr.at[j], device)

    def p_all(self, j):
        spot = self.pb.at[j, self.core, pl.ds(0, self.chips - 1)]
        return self.rcopy(spot, spot, self.ps.at[j], self.pr.at[j], self.partner)

    def p_share_copy(self, j, landing):
        core = lax.rem(self.core + 1, cores) if landing else self.core
        spot = self.pb.at[j, core]
        return self.rcopy(spot, spot, self.pds.at[j], self.pdr.at[j], self.partner)

    def p_share(self, j):
        self.p_all(j).wait_recv()
        self.p_share_copy(j, False).start()

    def s_copy(self, j, q, up):
        landing, recv = (self.lo, self.lr) if up else (self.hi, self.hr)
        return self.rcopy(
            self.sb.at[j, q], landing.at[j, q], self.ss.at[j], recv.at[j, q],
            lax.rem(self.me + (self.group if up else self.n - self.group), self.n),
        )

    def s_all(self, j):
        most = pl.ds(0, planes - 1)
        return self.rcopy(
            self.sb.at[j, most], self.lo.at[j, most], self.ss.at[j], self.lr.at[j, 0], self.partner
        )

    def p_mix(self, j):
        self.p_share_copy(j, True).wait_recv()
        rows, width = self.pb.shape[-2:]
        mixed = jnp.dot(
            self.m2[...], self.pb[j].reshape(-1, width), preferred_element_type=f32
        ).astype(bf16)
        self.sb[j] = mixed.reshape(planes, rows, width)
        self.p_hop(j, 0)

    def p_hop(self, j, h):
        def send(q, up):
            if h > 0:
                copy = self.s_copy(j, q, up)
                copy.wait_recv()
                landing = self.lo if up else self.hi
                self.sb[j, q] = (self.sb[j, q].astype(f32) + landing[j, q].astype(f32)).astype(bf16)
            self.s_copy(j, q, up).start()

        @pl.when(self.plane == h)
        def _():
            for q in range(planes - 1, h, -1):
                send(q, True)

        @pl.when(self.plane == planes - 1 - h)
        def _():
            for q in range(planes - 1 - h):
                send(q, False)

    def p_take(self, j, total):
        q = self.plane
        total[...] = self.sb[j, q].astype(f32)
        for up in (True, False):

            @pl.when(q > 0 if up else q + 1 < planes)
            def _():
                self.s_copy(j, q, up).wait_recv()
                total[...] += (self.lo if up else self.hi)[j, q].astype(f32)

    def run(self, fill, take_z, take_p):
        z, p = self.z_hop, self.p_hop
        assert steps == 4 and planes == 4
        z(0, 1); z(1, 1)
        fill()
        self.p_share(0)
        z(2, 1); z(3, 1)
        self.p_mix(0)
        z(0, 2); z(1, 2)
        self.p_share(1)
        z(2, 2); z(3, 2)
        self.p_mix(1)
        self.p_share(2)
        p(0, 1)
        z(0, 3); self.z_share(0)
        z(1, 3); self.z_share(1)
        self.p_mix(2)
        self.p_share(3)
        z(2, 3); self.z_share(2)
        self.z_mix(0)
        z(3, 3); self.z_share(3)
        p(1, 1)
        self.p_mix(3)
        self.z_mix(1)
        p(0, 2)
        self.z_mix(2)
        p(2, 1)
        self.z_mix(3)
        p(1, 2)
        p(3, 1)
        p(2, 2)
        take_z(0); take_z(1)
        p(3, 2)
        take_z(2); take_z(3)
        for j in range(steps):
            take_p(j)

    def drain(self):
        for j in range(steps):
            for up in (True, False):
                open_end = self.plane + 1 < planes if up else self.plane > 0
                for h in range(planes):
                    origin = self.plane - h if up else self.plane + h

                    @pl.when(open_end & (origin >= 0 if up else origin < planes))
                    def _():
                        self.z_copy(j, origin, up).wait_send()

            self.z_share_copy(j, False).wait_send()
            self.p_share_copy(j, False).wait_send()
            self.o_all(j).wait_send()
            self.p_all(j).wait_send()
            self.s_all(j).wait_send()


def exchange_scratch(n, rows, width):
    group = n // planes
    chips = group // cores
    part = width // (2 * steps)
    dma = lambda *count: pltpu.SemaphoreType.DMA(count)
    held = lambda *lead: pltpu.VMEM((steps, *lead, rows, part), bf16)
    return [
        held(cores, planes), held(chips), held(chips), held(cores, chips),
        held(planes), held(planes), held(planes),
        pltpu.VMEM((chips * rows, cores * planes * rows), bf16),
        pltpu.VMEM((planes * rows, cores * chips * rows), bf16),
        dma(steps, 2 * planes), dma(steps, planes), dma(steps), dma(steps), dma(steps), dma(steps),
        dma(steps), dma(steps), dma(steps), dma(steps), dma(steps),
        dma(steps, planes), dma(steps, planes),
    ]


exchange_refs = 22
input_count = 19
output_count = 3


def layer_kernel(n, limit, top, *refs):
    (
        tokens_h, conv_h, recur_h, wb_h, wg_h, taps_h, rate_h, input_h, decay_h, wm_h,
        g_pre_h, g_post_h, g_ffn_h, g_out_h, routes_h, affinity_h, eg_h, eu_h, ed_h,
    ) = refs[:input_count]
    out_h, branch_h, state_h = refs[input_count : input_count + output_count]
    refs = refs[input_count + output_count :]
    (
        tokens, conv_in, recur, wb, wg, taps, rate_b, input_b, decay_p, wm,
        g_pre, g_post, g_ffn, g_out, routes, affinity, eg, eu, ed,
    ) = refs[:input_count]
    refs = refs[input_count:]
    first = Exchange(n, refs[:exchange_refs])
    second = Exchange(n, refs[exchange_refs : 2 * exchange_refs])
    (
        out, branch_out, state_out, normed, gate_act, merged, mix, residual, message, mall,
        codes, base, share_at, sums_g, sums_u, total, hidden,
        load_sem, tile_sem, save_sem, ms, mr,
    ) = refs[2 * exchange_refs :]
    me, group, chips = first.me, first.group, first.chips
    plane, chip, core = first.plane, first.chip, first.core
    rows, width = tokens.shape
    channels = recur.shape[1]
    block = rate_b.shape[1]
    part = width // (2 * steps)
    wide = width // tile
    narrow = channels // tile

    sources = dict(
        tokens=(tokens_h, tokens), g_pre=(g_pre_h, g_pre), routes=(routes_h, routes),
        affinity=(affinity_h, affinity), conv=(conv_h, conv_in), taps=(taps_h, taps),
        rate=(rate_h, rate_b), input=(input_h, input_b), decay=(decay_h, decay_p),
        recur=(recur_h, recur), g_post=(g_post_h, g_post), g_ffn=(g_ffn_h, g_ffn),
        g_out=(g_out_h, g_out), eg=(eg_h.at[0], eg), eu=(eu_h.at[0], eu), ed=(ed_h.at[0], ed),
    )
    load = {
        name: pltpu.make_async_copy(src, dst, load_sem.at[k])
        for k, (name, (src, dst)) in enumerate(sources.items())
    }

    def strip(src, dst, t, k):
        cols = pl.ds(t * tile, tile)
        return pltpu.make_async_copy(src.at[:, cols], dst.at[:, cols], tile_sem.at[k])

    strips_b = [strip(wb_h, wb, t, t) for t in range(narrow)]
    strips_g = [strip(wg_h, wg, t, narrow + t) for t in range(narrow)]
    strips_m = [strip(wm_h, wm, t, 2 * narrow + t) for t in range(wide)]
    barrier = pltpu.get_barrier_semaphore()

    for name in ("tokens", "g_pre", "routes", "affinity"):
        load[name].start()
    for copy in strips_b:
        copy.start()

    @pl.loop(1, n)
    def _(d):
        pl.semaphore_signal(barrier, inc=1, device_id={"ep": lax.rem(me + d, n)})

    for copy in strips_g:
        copy.start()
    for name in ("conv", "taps", "rate", "input", "decay", "recur"):
        load[name].start()
    for copy in strips_m:
        copy.start()
    for name in ("g_post", "g_ffn", "g_out", "eg", "eu", "ed"):
        load[name].start()

    def lanes(k):
        return pl.ds(pl.multiple_of(k * lane, lane), lane)

    def message_copy(d, landing):
        device = lax.rem(me + d, n)
        spot = device if landing else me
        return pltpu.make_async_remote_copy(
            src_ref=message, dst_ref=mall.at[:, lanes(spot)], send_sem=ms.at[device],
            recv_sem=mr.at[spot], device_id={"ep": device},
            device_id_type=pl.DeviceIdType.MESH,
        )

    message[...] = jnp.full(message.shape, -1.0, f32)
    load["routes"].wait()
    load["affinity"].wait()
    message[:top, :rows] = routes[...].astype(f32)
    message[top : 2 * top, :rows] = affinity[...]
    mall[:, lanes(me)] = message[...]
    load["tokens"].wait()
    load["g_pre"].wait()
    normed[...] = rms(tokens[...].astype(f32), g_pre[...]).astype(bf16)

    def project(copies, weights, t):
        copies[t].wait()
        return jnp.dot(
            normed[...], weights[:, t * tile : (t + 1) * tile], preferred_element_type=f32
        ).astype(bf16)

    for t in range(narrow):
        branch_out[:, t * tile : (t + 1) * tile] = project(strips_b, wb, t)
    save_branch = pltpu.make_async_copy(branch_out, branch_h, save_sem.at[0])
    save_branch.start()
    pl.semaphore_wait(barrier, n - 1)

    @pl.loop(1, n)
    def _(d):
        message_copy(d, False).start()

    for t in range(narrow):
        gate_act[:, t * tile : (t + 1) * tile] = project(strips_g, wg, t)
    for name in ("conv", "taps", "rate", "input", "decay", "recur"):
        load[name].wait()

    same = iota((tile, tile), 0) // block == iota((tile, tile), 1) // block

    def spread(ref, t):
        piece = ref[pl.ds(t * tile, tile), :].astype(f32)
        return jnp.where(same, jnp.concatenate([piece] * (tile // block), axis=1), 0.0).astype(bf16)

    past = conv_in.shape[0]
    for t in range(narrow):
        cols = slice(t * tile, (t + 1) * tile)
        conv = branch_out[:, cols].astype(f32) * taps[past : past + 1, cols]
        for k in range(past):
            conv = conv + conv_in[k, :, cols].astype(f32) * taps[k : k + 1, cols]
        conv16 = conv.astype(bf16)
        rate = jax.nn.sigmoid(jnp.dot(conv16, spread(rate_b, t), preferred_element_type=f32))
        inflow = jax.nn.sigmoid(jnp.dot(conv16, spread(input_b, t), preferred_element_type=f32))
        log_decay = rate * (-gate_scale * jax.nn.softplus(-decay_p[:, cols]))
        decay = jnp.exp(log_decay)
        rest = -jnp.tanh(log_decay) * (decay * decay + 1.0)
        state = decay * recur[:, cols] + jnp.sqrt(rest) * (inflow * conv)
        state_out[:, cols] = state
        merged[:, cols] = (state * jax.nn.gelu(gate_act[:, cols].astype(f32))).astype(bf16)
    save_state = pltpu.make_async_copy(state_out, state_h, save_sem.at[1])
    save_state.start()

    for t in range(wide):
        strips_m[t].wait()
        cols = slice(t * tile, (t + 1) * tile)
        mix[:, cols] = (
            jnp.dot(merged[...], wm[:, cols], preferred_element_type=f32).astype(bf16).astype(f32)
        )
    for name in ("g_post", "g_ffn", "g_out"):
        load[name].wait()
    residual[...] = tokens[...].astype(f32) + rms(mix[...], g_post[...])
    ffn = rms(residual[...], g_ffn[...]).astype(bf16)

    def feature(half, j):
        start = (half * steps + j) * part
        return slice(start, start + part)

    for j in range(steps):
        first.put_z(j, ffn[:, feature(0, j)])
        first.put_p(j, ffn[:, feature(1, j)])

    @pl.loop(1, n)
    def _(d):
        message_copy(d, True).wait_recv()

    names = iota((n, 1), 0).astype(f32)
    left, right = iota((lane, 2 * lane), 0), iota((lane, 2 * lane), 1)
    ladder = jnp.where((left < right) | (right >= lane), 1.0, 0.0).astype(bf16)
    batch = min(n, max(1, 1024 // n))
    base[...] = jnp.zeros(base.shape, f32)

    def rank_batch(b):
        tiles = [mall[:, lanes(b * batch + i)] for i in range(batch)]
        hot = [[jnp.where(v[k : k + 1] == names, 1.0, 0.0) for k in range(top)] for v in tiles]
        counts = jnp.dot(
            jnp.concatenate([sum(h) for h in hot], axis=0).astype(bf16), ladder,
            preferred_element_type=f32,
        )
        running = base[...]
        for i in range(batch):
            count = counts[i * n : (i + 1) * n]
            place = running + count[:, :lane]
            running = running + count[:, lane:]
            raw = [tiles[i][top + k : top + k + 1] for k in range(top)]
            for k in range(top):
                rank = jnp.sum(hot[i][k] * place, axis=0, keepdims=True)
                code = jnp.where(rank < limit, tiles[i][k : k + 1] * limit + rank, -1.0)
                codes[k : k + 1, lanes(b * batch + i)] = code
                codes[top + k : top + k + 1, lanes(b * batch + i)] = raw[k] / sum(raw)
        base[...] = running

    if batch == n:
        rank_batch(0)
    else:
        pl.loop(0, n // batch)(rank_batch)

    def codes_of(devices):
        return jnp.concatenate([codes[:, lanes(d)][:, :rows] for d in devices], axis=1)

    def device_of(q, c, k):
        return q * group + c * cores + k

    along = [device_of(q, chip, k) for k in range(cores) for q in range(planes)]
    around = [device_of(plane, c, k) for k in range(cores) for c in range(chips)]
    mine_around = [device_of(plane, c, core) for c in range(chips)]
    mine_along = [device_of(q, chip, core) for q in range(planes)]

    def slots_of(devices, dim):
        spot = iota((1, rows) if dim else (rows, 1), dim)
        return jnp.concatenate([(d * limit + spot).astype(f32) for d in devices], axis=dim)

    def match(at_rows, at_lanes):
        hit = jnp.zeros((at_rows[0].shape[0], at_lanes[0].shape[1]), f32)
        for r in at_rows:
            for v in at_lanes:
                hit = jnp.where(r == v, 1.0, hit)
        return hit.astype(bf16)

    def split(block_of):
        return [block_of[k : k + 1] for k in range(top)]

    first.m2[...] = match([slots_of(mine_along, 0)], split(codes_of(around)))
    first.m1[...] = match([slots_of(mine_around, 0)], split(codes_of(along)))

    def fill_back():
        for m, targets, sources_of in (
            (second.m1, mine_around, along), (second.m2, mine_along, around)
        ):
            turned = jnp.transpose(codes_of(targets))
            m[...] = match(
                [turned[:, k : k + 1] for k in range(top)], [slots_of(sources_of, 1)]
            )
        share_at[...] = jnp.zeros(share_at.shape, f32)
        wanted = (me * limit + iota((rows, 1), 0)).astype(f32)

        def add_shares(b):
            found = share_at[...]
            for i in range(8):
                v = codes[:, lanes(b * 8 + i)]
                for k in range(top):
                    found = found + jnp.where(v[k : k + 1] == wanted, v[top + k : top + k + 1], 0.0)
            share_at[...] = found

        pl.loop(0, n // 8)(add_shares)

    started = [False]

    def absorb(half, j, x):
        if not started[0]:
            load["eg"].wait()
            load["eu"].wait()
        for w, sums in ((eg, sums_g), (eu, sums_u)):
            piece = jnp.dot(x, w[feature(half, j), :], preferred_element_type=f32)
            sums[...] = sums[...] + piece if started[0] else piece
        started[0] = True

    def take_z(j):
        absorb(0, j, first.z_take(j).astype(bf16))

    def take_p(j):
        first.p_take(j, total.at[0])
        absorb(1, j, total[0].astype(bf16))

    first.run(fill_back, take_z, take_p)

    hidden[...] = (jax.nn.silu(sums_g[...]) * sums_u[...]).astype(bf16)
    share = jnp.sum(share_at[...], axis=1, keepdims=True)
    load["ed"].wait()

    def expert_out(half, j):
        made = jnp.dot(hidden[...], ed[:, feature(half, j)], preferred_element_type=f32)
        return (made.astype(bf16).astype(f32) * share).astype(bf16)

    for j in range(steps):
        second.put_z(j, expert_out(0, j))
        second.put_p(j, expert_out(1, j))

    def keep_z(j):
        total[j] = second.z_take(j)

    def keep_p(j):
        second.p_take(j, total.at[steps + j])

    second.run(lambda: None, keep_z, keep_p)

    squares = jnp.zeros((rows, 1), f32)
    for c in range(2 * steps):
        squares = squares + jnp.sum(total[c] * total[c], axis=1, keepdims=True)
    scale = lax.rsqrt(squares / width + epsilon)
    for c in range(2 * steps):
        cols = slice(c * part, (c + 1) * part)
        out[:, cols] = (residual[:, cols] + total[c] * scale * g_out[:, cols]).astype(out.dtype)
    save_out = pltpu.make_async_copy(out, out_h, save_sem.at[2])
    save_out.start()

    @pl.loop(1, n)
    def _(d):
        message_copy(d, False).wait_send()

    first.drain()
    second.drain()
    save_branch.wait()
    save_state.wait()
    save_out.wait()


def finish_kernel(out_i, branch_i, state_i, conv_i, out_o, conv_o, state_o, ob, cb, sb, sems):
    past = conv_i.shape[0]
    ins = [
        pltpu.make_async_copy(conv_i.at[pl.ds(1, past - 1)], cb.at[pl.ds(0, past - 1)], sems.at[0]),
        pltpu.make_async_copy(branch_i, cb.at[past - 1], sems.at[1]),
        pltpu.make_async_copy(state_i, sb, sems.at[2]),
        pltpu.make_async_copy(out_i, ob, sems.at[3]),
    ]
    outs = [
        pltpu.make_async_copy(cb, conv_o, sems.at[4]),
        pltpu.make_async_copy(sb, state_o, sems.at[5]),
        pltpu.make_async_copy(ob, out_o, sems.at[6]),
    ]
    for copy in ins:
        copy.start()
    ins[0].wait()
    ins[1].wait()
    outs[0].start()
    ins[2].wait()
    outs[1].start()
    ins[3].wait()
    outs[2].start()
    for copy in outs:
        copy.wait()


def anywhere(count):
    return [pl.BlockSpec(memory_space=pl.ANY)] * count


def shards(
    tokens, conv_state, recur_state, w_branch, w_gate, conv_taps, rate_blocks, input_blocks,
    decay_param, w_mix, gain_pre, gain_post, gain_ffn, gain_out, routes, affinity,
    w_expert_gate, w_expert_up, w_expert_down,
):
    n = lax.axis_size("ep")
    rows, width = tokens.shape
    channels = recur_state.shape[1]
    past = conv_state.shape[1]
    top = routes.shape[1]
    ff = w_expert_gate.shape[2]
    block = rate_blocks.shape[2]
    limit = rows * top // 2
    assert limit == rows

    row = lambda v: v.reshape(1, -1)
    dma = lambda *count: pltpu.SemaphoreType.DMA(count)
    letter = (-(-2 * top // 8) * 8, lane)
    conv_turned = jnp.transpose(conv_state, (1, 0, 2))
    operands = (
        tokens, conv_turned, recur_state, w_branch, w_gate, conv_taps,
        rate_blocks.reshape(channels, block), input_blocks.reshape(channels, block),
        row(decay_param), w_mix, row(gain_pre), row(gain_post), row(gain_ffn), row(gain_out),
        routes.T, affinity.T, w_expert_gate, w_expert_up, w_expert_down,
    )
    held = [pltpu.VMEM(v.shape[1:] if k >= 16 else v.shape, v.dtype) for k, v in enumerate(operands)]
    made, branch, state = pl.pallas_call(
        functools.partial(layer_kernel, n, limit, top),
        out_shape=(
            jax.ShapeDtypeStruct((rows, width), bf16),
            jax.ShapeDtypeStruct((rows, channels), bf16),
            jax.ShapeDtypeStruct((rows, channels), f32),
        ),
        in_specs=anywhere(input_count),
        out_specs=tuple(anywhere(output_count)),
        scratch_shapes=held
        + exchange_scratch(n, rows, width)
        + exchange_scratch(n, rows, width)
        + [
            pltpu.VMEM((rows, width), bf16),
            pltpu.VMEM((rows, channels), bf16),
            pltpu.VMEM((rows, channels), f32),
            pltpu.VMEM((rows, width), bf16),
            pltpu.VMEM((rows, channels), bf16),
            pltpu.VMEM((rows, channels), bf16),
            pltpu.VMEM((rows, width), f32),
            pltpu.VMEM((rows, width), f32),
            pltpu.VMEM(letter, f32),
            pltpu.VMEM((letter[0], n * lane), f32),
            pltpu.VMEM((letter[0], n * lane), f32),
            pltpu.VMEM((n, lane), f32),
            pltpu.VMEM((rows, lane), f32),
            pltpu.VMEM((rows, ff), f32),
            pltpu.VMEM((rows, ff), f32),
            pltpu.VMEM((2 * steps, rows, width // (2 * steps)), f32),
            pltpu.VMEM((rows, ff), bf16),
            dma(16), dma((2 * channels + width) // tile), dma(3), dma(n), dma(n),
        ],
        compiler_params=pltpu.CompilerParams(
            collective_id=0, has_side_effects=True, vmem_limit_bytes=60 << 20
        ),
    )(*operands)
    layer_out, conv_next, state_next = pl.pallas_call(
        finish_kernel,
        out_shape=(
            jax.ShapeDtypeStruct((rows, width), bf16),
            jax.ShapeDtypeStruct((past, rows, channels), bf16),
            jax.ShapeDtypeStruct((rows, channels), f32),
        ),
        in_specs=anywhere(4),
        out_specs=tuple(anywhere(3)),
        scratch_shapes=[
            pltpu.VMEM((rows, width), bf16),
            pltpu.VMEM((past, rows, channels), bf16),
            pltpu.VMEM((rows, channels), f32),
            dma(7),
        ],
    )(made, branch, state, conv_turned)
    return (layer_out, jnp.transpose(conv_next, (1, 0, 2)), state_next)


def solution(mesh):
    ep, copied = "ep", P()
    return jax.shard_map(
        shards,
        mesh=mesh,
        in_specs=(P(ep, None), P(ep, None, None), P(ep, None))
        + (copied,) * 11
        + (P(ep, None),) * 2
        + (P(ep, None, None),) * 3,
        out_specs=(P(ep, None), P(ep, None, None), P(ep, None)),
        check_vma=False,
    )
```

time: 87.7 us -> 61.5 us (0.70)
  Pallas kernels: 77.1 us -> 60.7 us
  local copies, waits for them, and re-layouts: 6.11 us -> 0 us
  other arithmetic: 3.49 us -> 0 us
    pallas_call x1 -> x2, Pallas kernels: 77.1 us -> 60.7 us  [the longest x1 58.8 us: shards(): pl.pallas_call(functools.partial(layer_kernel, n, limit, top), out_shape=...]
    unnamed x4 -> x0, local copies, waits for them, and re-layouts: 6.1 us -> none
    reduce_sum x1 -> x0, other arithmetic: 1.8 us -> none  [shards(): pre = jnp.sum(conv_state.astype(f32) * conv_taps[None, :-1], axis=1)]
    concatenate x1 -> x0, other arithmetic: 1.69 us -> none  [shards(): conv_next = jnp.concatenate([conv_state[:, 1:], branch[:, None, :]], axis=1)]
where the time goes in v1:
time: 61.5 us; the launch traced here: 61.4 us
  Pallas kernels  60.7 us (99%)
  between operations  0.65 us (1%)
    pallas_call x1, Pallas kernels, shards(): pl.pallas_call(functools.partial(layer_kernel, n, limit, top), out_shape=...  58.8 us
    pallas_call x1, Pallas kernels, shards(): pl.pallas_call(finish_kernel, out_shape=(jax.ShapeDtypeStruct((rows, widt...  1.97 us

profile of v1, /device:TPU:0, one launch (start us, length us, event | category | flops | bytes accessed | tf_op | source)
XLA Modules:
  0.0 61.4 jit_solution(5308342235652138304)
XLA Ops:
  0.6 58.8 %shard_map.202 = (bf16[64,2048]{1,0:T(8,128)(2,1)}, bf16[64,1024]{1,0:T(8,128)(2,1)}, f32[64,1024]{1,0:T(8,128)}) custom-call(bf16[64,2048]{1,0:T(8,128)(2,1)} %refs_0_.1, bf16[3,64,1024]{2,1,0:T(8,128)(2,1)} %bitcast.11, f32[64,1024]{1,0:T(8,128)} %refs_2_.1, bf16[2048,1024]{1,0:T(8,128)(2,1)} %refs_3_.1, bf16[2048,1024]{1,0:T(8,128)(2,1)} %refs_4_.1, ...), custom_call_target="tpu_custom_call" | custom-call | tf_op jit(solution)/shard_map/pallas_call | solution.py:625
  59.4 2.0 %shard_map.203 = (bf16[64,2048]{1,0:T(8,128)(2,1)}, bf16[3,64,1024]{2,1,0:T(8,128)(2,1)}, f32[64,1024]{1,0:T(8,128)}) custom-call(bf16[64,2048]{1,0:T(8,128)(2,1)} %get-tuple-element.9.out_i, bf16[64,1024]{1,0:T(8,128)(2,1)} %get-tuple-element.10.branch_i, f32[64,1024]{1,0:T(8,128)} %get-tuple-element.11.state_i, bf16[3,64,1024]{2,1,0:T(8,128)(2,1)} %bitcast.12), custom_call_target="tpu_custom_call" | custom-call | tf_op jit(solution)/shard_map/pallas_call | solution.py:661
